TPU v7x, 32 devices: a whole 2x2x4 slice. The times are simulated.
32 devices in a mesh: ep: 8 (over z, core), tp: 4 (over y, x).
Axes of the slice: x: 2, y: 2, z: 4, core: 2. Of those that a mesh axis runs over, the one named last changes fastest.
Arguments:
- tokens: bfloat16 [1024, 2048], P('ep'), may hold values from -6 to 6
- chosen: int32 [8, 8, 8], replicated, may hold values from 0 to 127, as said below
- chosen_weight: float32 [8, 8, 8], P('ep'), may hold values from 0.1 to 1
- gate_weight: bfloat16 [8, 2048, 4096], P('ep', None, 'tp'), may hold values from -0.125 to 0.125
- up_weight: bfloat16 [8, 2048, 4096], P('ep', None, 'tp'), may hold values from -0.125 to 0.125
- down_weight: bfloat16 [8, 4096, 2048], P('ep', 'tp'), may hold values from -0.09375 to 0.09375
Outputs:
- combined: bfloat16 [1024, 2048], P('ep', 'tp')
Inputs may be any that keep to these rules, and one draw needn't show every extreme that they name: `chosen`: for every block and expert the 8 positions are distinct.
All inputs are finite; a program needn't handle non-finite values.
Results may differ from a plain program's by a relative error of at most 0.015.
Values may be sent and summed in bfloat16 or wider, within the bound.
A program may use at most 64 MiB of HBM per device.

v0:
```python
import jax
import jax.numpy as jnp
from jax import lax
from jax.sharding import PartitionSpec as P


def local(tokens, chosen, chosen_weight, gate_weight, up_weight, down_weight):
    ep_index = lax.axis_index("ep")
    tp_count = lax.axis_size("tp")
    tp_index = lax.axis_index("tp")
    tok_count, model_width = tokens.shape
    blocks, experts, picks_each = chosen.shape
    slice_width = model_width // tp_count
    columns = lax.dynamic_slice_in_dim(tokens, tp_index * slice_width, slice_width, 1)
    outgoing = lax.dynamic_index_in_dim(chosen, ep_index, 0, keepdims=False)
    leaving = jnp.take(columns, outgoing.reshape(-1), axis=0).reshape(
        experts, picks_each, slice_width
    )
    arrived = lax.all_to_all(leaving, "ep", split_axis=0, concat_axis=0, tiled=True).reshape(
        blocks * picks_each, slice_width
    )
    gate_local = gate_weight[0]
    up_local = up_weight[0]
    portion = lax.all_gather(arrived, "tp", axis=1, tiled=True)
    gate_sum = jnp.dot(portion, gate_local, preferred_element_type=jnp.float32)
    up_sum = jnp.dot(portion, up_local, preferred_element_type=jnp.float32)
    hidden = (jax.nn.silu(gate_sum) * up_sum).astype(jnp.bfloat16)
    down_local = down_weight[0].reshape(down_weight.shape[1], tp_count, slice_width)
    summed = lax.psum_scatter(
        jnp.einsum("rf,fcd->crd", hidden, down_local, preferred_element_type=jnp.float32).astype(
            jnp.bfloat16
        ),
        "tp",
        scatter_dimension=0,
        tiled=True,
    ).astype(jnp.float32)
    expert_out = summed[0].astype(jnp.bfloat16).reshape(blocks, picks_each, slice_width)
    returned = lax.all_to_all(expert_out, "ep", split_axis=0, concat_axis=0, tiled=True).reshape(
        experts * picks_each, slice_width
    )
    positions = jnp.arange(tok_count, dtype=jnp.int32)[:, None]
    placement_matrix = jnp.where(
        outgoing.reshape(1, -1) == positions, chosen_weight[0].reshape(1, -1), 0.0
    )
    combined = jnp.dot(
        placement_matrix,
        returned.astype(jnp.float32),
        precision=lax.Precision.HIGHEST,
        preferred_element_type=jnp.float32,
    )
    return combined.astype(jnp.bfloat16)


def solution(mesh):
    return jax.shard_map(
        local,
        mesh=mesh,
        in_specs=(
            P("ep", None),
            P(),
            P("ep", None, None),
            P("ep", None, "tp"),
            P("ep", None, "tp"),
            P("ep", "tp", None),
        ),
        out_specs=P("ep", "tp"),
        check_vma=False,
    )
```

profile of v0, /device:TPU:0, one launch (start us, length us, event | category | flops | bytes accessed | tf_op | source)
XLA Modules:
  0.0 84.8 jit_solution(2384732761228838541)
XLA Ops:
  6.5 0.0 copy-start
  6.5 0.8 compare_and_fusion
  7.3 0.1 reshape.58
  7.4 0.2 copy-done
  7.6 0.7 gather_fusion
  8.3 0.7 bitcast_select_fusion
  9.0 6.4 %all-to-all-start = ((bf16[8,8,512]{2,1,0:T(8,128)(2,1)}), bf16[8,8,512]{2,1,0:T(8,128)(2,1)S(1)}, u32[]{:S(2)}, u32[]{:S(2)}) async-start(bf16[8,8,512]{2,1,0:T(8,128)(2,1)} %bitcast_select_fusion), calls=%async_computation | async-start | bytes 131072 | tf_op jit(solution)/shard_map/all_to_all | solution.py:19
  15.4 0.0 reduce-scatter.4.cloned.1.call-start
  15.4 7.8 %reshape_squeeze.4 = bf16[1024,4,512]{2,1,0:T(4,128)(2,1)} reshape(bf16[1,1024,2048]{2,1,0:T(8,128)(2,1)} %param.11) | data formatting | bytes 8388608 | tf_op jit(solution)/shard_map/reshape;squeeze | solution.py:28
  23.2 0.0 all-to-all-done
  23.2 9.0 %all_gather.3 = bf16[64,2048]{1,0:T(8,128)(2,1)S(1)} all-gather(bf16[64,512]{1,0:T(8,128)(2,1)S(1)} %bitcast.36), channel_id=1, replica_groups=mesh['ep'=8,'tp'=4] {'tp'}, dimensions={1}, use_global_device_ids=true | all-gather | bytes 327680 | tf_op jit(solution)/shard_map/all_gather | solution.py:24
  32.2 3.0 %fusion.2 = f32[64,1024]{1,0:T(8,128)S(1)} fusion(bf16[64,2048]{1,0:T(8,128)(2,1)S(1)} %all_gather.3, bf16[1,2048,1024]{2,1,0:T(8,128)(2,1)} %param.9), kind=kOutput, calls=%fused_computation.3 | convolution fusion | flops 268435456 | bytes 4718592 | tf_op jit(solution)/shard_map/dot_general | solution.py:25
  35.2 0.0 copy-start.1
  35.2 6.3 %fusion.12 = bf16[4,64,512]{2,1,0:T(8,128)(2,1)} fusion(bf16[1024,4,512]{2,1,0:T(4,128)(2,1)} %reshape_squeeze.4, bf16[64,2048]{1,0:T(8,128)(2,1)S(1)} %all_gather.3, bf16[1,2048,1024]{2,1,0:T(8,128)(2,1)} %param.10, f32[64,1024]{1,0:T(8,128)S(1)} %fusion.2), kind=kOutput, calls=%fused_computation.9 | convolution fusion | flops 537395200 | bytes 9175040 | tf_op jit(solution)/shard_map/rf,fcd->crd/dot_general | solution.py:30
  41.6 0.0 reduce-scatter.4.cloned.1.call-update
  41.6 25.0 %reduce-scatter.4.cloned.1.call-done = bf16[1,64,512]{2,1,0:T(8,128)(2,1)} async-done(((bf16[4,64,512]{2,1,0:T(8,128)(2,1)}), bf16[1,64,512]{2,1,0:T(8,128)(2,1)}) %reduce-scatter.4.cloned.1.call-update) | async-done | bytes 65552
  66.6 4.6 %all-to-all-start.1 = ((bf16[8,8,512]{2,1,0:T(8,128)(2,1)}), bf16[8,8,512]{2,1,0:T(8,128)(2,1)S(1)}, u32[]{:S(2)}, u32[]{:S(2)}) async-start(bf16[8,8,512]{2,1,0:T(8,128)(2,1)} %bitcast.37), calls=%async_computation.1 | async-start | bytes 131072 | tf_op jit(solution)/shard_map/all_to_all | solution.py:38
  71.2 0.1 eq.17
  71.3 0.0 copy-done.1
  71.3 0.1 broadcast_in_dim.25
  71.3 5.8 %all-to-all-done.1 = bf16[8,8,512]{2,1,0:T(8,128)(2,1)S(1)} async-done(((bf16[8,8,512]{2,1,0:T(8,128)(2,1)}), bf16[8,8,512]{2,1,0:T(8,128)(2,1)S(1)}, u32[]{:S(2)}, u32[]{:S(2)}) %all-to-all-start.1) | async-done | bytes 65568 | tf_op jit(solution)/shard_map/all_to_all | solution.py:38
  77.1 0.9 %convolution_convert_fusion = bf16[128,512]{1,0:T(8,128)(2,1)} fusion(bf16[8,8,512]{2,1,0:T(8,128)(2,1)S(1)} %all-to-all-done.1, f32[64]{0:T(128)S(1)} %broadcast_in_dim.25, s32[64]{0:T(128)S(1)} %eq.17), kind=kOutput, calls=%fused_computation.11 | convolution fusion | flops 50413568 | bytes 197120 | tf_op jit(solution)/shard_map/dot_general | solution.py:45
  (3 shorter events, 0.0 us)
Async XLA Ops:
  6.5 1.1 %copy-start = (bf16[128,2048]{1,0:T(8,128)(2,1)S(1)}, bf16[128,2048]{1,0:T(8,128)(2,1)}, u32[]{:S(2)}) copy-start(bf16[128,2048]{1,0:T(8,128)(2,1)} %param.6) | copy-start | bytes 1572868
  9.0 14.2 %all-to-all-start = ((bf16[8,8,512]{2,1,0:T(8,128)(2,1)}), bf16[8,8,512]{2,1,0:T(8,128)(2,1)S(1)}, u32[]{:S(2)}, u32[]{:S(2)}) async-start(bf16[8,8,512]{2,1,0:T(8,128)(2,1)} %bitcast_select_fusion), calls=%async_computation | async-start | bytes 131072 | tf_op jit(solution)/shard_map/all_to_all | solution.py:19
  15.4 51.2 %reduce-scatter.4.cloned.1.call-start = ((), (), s32[]{:S(2)}) async-start(), calls=%async_computation.3 | async-start | bytes 327680
  35.2 36.0 %copy-start.1 = (f32[1,8,8]{2,1,0:T(8,128)S(1)}, f32[1,8,8]{2,1,0:T(8,128)}, u32[]{:S(2)}) copy-start(f32[1,8,8]{2,1,0:T(8,128)} %param.8) | copy-start | bytes 772
  66.6 10.5 %all-to-all-start.1 = ((bf16[8,8,512]{2,1,0:T(8,128)(2,1)}), bf16[8,8,512]{2,1,0:T(8,128)(2,1)S(1)}, u32[]{:S(2)}, u32[]{:S(2)}) async-start(bf16[8,8,512]{2,1,0:T(8,128)(2,1)} %bitcast.37), calls=%async_computation.1 | async-start | bytes 131072 | tf_op jit(solution)/shard_map/all_to_all | solution.py:38
Sparse Core Ops, SparseCore 0:
  41.7 24.7 reduce-scatter.3
where the time goes:
time: 85.3 us; the launch traced here: 84.8 us
  waiting for transfers between devices  30.7 us (36%)
  between operations  13.4 us (16%)
  starting transfers between devices  11 us (13%)
  matrix products  10.3 us (12%)
  blocking collectives  8.98 us (11%)
  local copies, waits for them, and re-layouts  8.96 us (11%)
  other arithmetic  1.48 us (2%)
    unnamed x2, waiting for transfers between devices  25 us
    all_gather x1, blocking collectives, local(): portion = lax.all_gather(arrived, 'tp', axis=1, tiled=True)  8.98 us
    another operation x1, local copies, waits for them, and re-layouts, local(): down_weight[0].reshape(down_weight.shape[1], tp_count, slice_width)  7.8 us
    all_to_all x1, starting transfers between devices, local(): lax.all_to_all(leaving, 'ep', split_axis=0, concat_axis=0, tiled=True)  6.35 us
    dot_general x1, matrix products, local(): jnp.einsum('rf,fcd->crd', hidden, down_local, preferred_element_type=jnp....  6.33 us
    all_to_all x1, waiting for transfers between devices, local(): lax.all_to_all(expert_out, 'ep', split_axis=0, concat_axis=0, tiled=True)  5.76 us
    all_to_all x1, starting transfers between devices, local(): lax.all_to_all(expert_out, 'ep', split_axis=0, concat_axis=0, tiled=True)  4.61 us
    dot_general x1, matrix products, local(): gate_sum = jnp.dot(portion, gate_local, preferred_element_type=jnp.float32)  3.03 us
  transfers between devices with their start and end apart: 3, of which 2 were waited for; matrix products, arithmetic and copies ran while one was open for 9% of the time, Pallas kernels for 0%

commit v1 on v0

v1 whole, which is shorter than its diff:
```python
import functools

import jax
import jax.numpy as jnp
from jax import lax
from jax.experimental import pallas as pl
from jax.experimental.pallas import tpu as pltpu
from jax.sharding import PartitionSpec as P

MESH = pl.DeviceIdType.MESH
CHUNKS = 4


def each(count, body):
    if count <= 8:
        for i in range(count):
            body(i)
    else:
        pl.loop(0, count)(body)


def partner(t, j, count):
    if count & (count - 1):
        return lax.rem(t + j, count)
    out, bit = 0, 1
    while bit < count:
        have = (t // bit) % 2
        out = out + ((have + 1) % 2 if j & bit else have) * bit
        bit *= 2
    return out


def kernel(
    n_ep, n_tp,
    tok_hbm, cho_hbm, wt_hbm, gate_hbm, up_hbm, down_hbm,
    out_ref,
    tok, cho, wt, gate, up, down,
    leaving, arrived, gate_acc, up_acc, place,
    part_out, part_in, back_out, back_in,
    in_sem, w_sem, d_sem,
    s1_send, s1_recv, s2_send, s2_recv, s3_send, s3_recv,
):
    e = lax.axis_index("ep")
    t = lax.axis_index("tp")
    tok_count, width = tok.shape
    experts, picks = cho.shape
    rows = experts * picks
    cw = width // CHUNKS
    sw = width // n_tp
    hid = gate.shape[1]

    def ep_peer(j):
        low = n_ep - 1 - j
        low = jnp.where(low > e, low, low - 1)
        high = jnp.where(j < e, j, j + 1)
        return jnp.where(e < n_ep // 2, low, high)

    barrier = pltpu.get_barrier_semaphore()

    def greet(j):
        pl.semaphore_signal(barrier, inc=1, device_id={"ep": ep_peer(j)}, device_id_type=MESH)

    each(n_ep - 1, greet)
    for j in range(1, n_tp):
        pl.semaphore_signal(
            barrier, inc=1, device_id={"tp": partner(t, j, n_tp)}, device_id_type=MESH
        )

    loads = [
        pltpu.make_async_copy(cho_hbm.at[e], cho, in_sem.at[0]),
        pltpu.make_async_copy(wt_hbm.at[0], wt, in_sem.at[1]),
        pltpu.make_async_copy(tok_hbm, tok, in_sem.at[2]),
    ]
    for c in loads:
        c.start()
    wloads = []
    for k in range(CHUNKS):
        piece = pl.ds(k * cw, cw)
        a = pltpu.make_async_copy(gate_hbm.at[0, piece, :], gate.at[piece, :], w_sem.at[0, k])
        b = pltpu.make_async_copy(up_hbm.at[0, piece, :], up.at[piece, :], w_sem.at[1, k])
        a.start()
        b.start()
        wloads.append((a, b))
    order = [*range(n_tp - 1, 0, -1), 0]
    dloads = {}
    for j in order:
        col = pl.multiple_of(partner(t, j, n_tp) * sw, sw)
        dloads[j] = pltpu.make_async_copy(
            down_hbm.at[0, :, pl.ds(col, sw)], down.at[j], d_sem.at[j]
        )
        dloads[j].start()

    for c in loads:
        c.wait()
    lane = lax.broadcasted_iota(jnp.int32, (picks, picks), 1)
    sub = lax.broadcasted_iota(jnp.int32, (picks, picks), 0)
    diag = lane == sub
    position = lax.broadcasted_iota(jnp.int32, (picks, tok_count), 1).astype(jnp.float32)
    hots, parts = [], []
    for x in range(experts):
        spread = jnp.broadcast_to(cho[x : x + 1, :], (picks, picks)).astype(jnp.float32)
        column = jnp.sum(jnp.where(diag, spread, 0.0), axis=1, keepdims=True)
        wide = jnp.broadcast_to(wt[x : x + 1, :], (picks, picks))
        wcol = jnp.sum(jnp.where(diag, wide, 0.0), axis=1, keepdims=True)
        hit = position == column
        hots.append(jnp.where(hit, 1.0, 0.0))
        parts.append(jnp.where(hit, wcol, 0.0))
    onehot = jnp.concatenate(hots, axis=0).astype(jnp.bfloat16)
    for k in range(CHUNKS):
        sel = jnp.dot(
            onehot, tok[:, k * cw : (k + 1) * cw], preferred_element_type=jnp.float32
        )
        leaving[k] = sel.reshape(experts, picks, cw).astype(jnp.bfloat16)

    pl.semaphore_wait(barrier, n_ep - 1 + n_tp - 1)

    def send_tokens(k, j):
        p = ep_peer(j)
        return pltpu.make_async_remote_copy(
            src_ref=leaving.at[k, p],
            dst_ref=arrived.at[k, e],
            send_sem=s1_send.at[k, j],
            recv_sem=s1_recv.at[k, e],
            device_id={"ep": p},
            device_id_type=MESH,
        )

    for k in range(CHUNKS):
        each(n_ep - 1, lambda j: send_tokens(k, j).start())

    weighted = jnp.concatenate(parts, axis=0)
    hi = weighted.astype(jnp.bfloat16).astype(jnp.float32)
    mid = (weighted - hi).astype(jnp.bfloat16).astype(jnp.float32)
    lo = weighted - hi - mid
    for i, piece in enumerate((hi, mid, lo)):
        place[i] = piece.T.astype(jnp.bfloat16)

    def rows_in(ref, k, sem, p):
        pltpu.make_async_remote_copy(
            src_ref=ref.at[k, p] if k is not None else ref.at[p],
            dst_ref=ref.at[k, p] if k is not None else ref.at[p],
            send_sem=sem.at[k, p] if k is not None else sem.at[p],
            recv_sem=sem.at[k, p] if k is not None else sem.at[p],
            device_id={"ep": p},
            device_id_type=MESH,
        ).wait_recv()

    for k in range(CHUNKS):
        arrived[k, e] = leaving[k, e]
        each(n_ep - 1, lambda j: rows_in(arrived, k, s1_recv, ep_peer(j)))
        x = arrived[k].astype(jnp.float32).reshape(rows, cw).astype(jnp.bfloat16)
        for c in wloads[k]:
            c.wait()
        g = jnp.dot(x, gate[k * cw : (k + 1) * cw, :], preferred_element_type=jnp.float32)
        u = jnp.dot(x, up[k * cw : (k + 1) * cw, :], preferred_element_type=jnp.float32)
        if k == 0:
            gate_acc[...] = g
            up_acc[...] = u
        else:
            gate_acc[...] += g
            up_acc[...] += u
    g = gate_acc[...]
    hidden = (g / (1.0 + jnp.exp(-g)) * up_acc[...]).astype(jnp.bfloat16)

    sends = []
    for j in order:
        dloads[j].wait()
        part_out[j] = jnp.dot(hidden, down[j], preferred_element_type=jnp.float32).astype(
            jnp.bfloat16
        )
        if j:
            c = pltpu.make_async_remote_copy(
                src_ref=part_out.at[j],
                dst_ref=part_in.at[j - 1],
                send_sem=s2_send.at[j - 1],
                recv_sem=s2_recv.at[j - 1],
                device_id={"tp": partner(t, j, n_tp)},
                device_id_type=MESH,
            )
            c.start()
            sends.append(c)
    total = part_out[0].astype(jnp.float32)
    for c in sends:
        c.wait_recv()
    for j in range(1, n_tp):
        total += part_in[j - 1].astype(jnp.float32)
    back_out[...] = total.reshape(n_ep, picks, sw).astype(jnp.bfloat16)

    def send_back(j):
        p = ep_peer(j)
        return pltpu.make_async_remote_copy(
            src_ref=back_out.at[p],
            dst_ref=back_in.at[e],
            send_sem=s3_send.at[j],
            recv_sem=s3_recv.at[e],
            device_id={"ep": p},
            device_id_type=MESH,
        )

    each(n_ep - 1, lambda j: send_back(j).start())
    back_in[e] = back_out[e]
    each(n_ep - 1, lambda j: rows_in(back_in, None, s3_recv, ep_peer(j)))
    y = back_in[...].astype(jnp.float32).reshape(rows, sw).astype(jnp.bfloat16)
    result = jnp.dot(place[0], y, preferred_element_type=jnp.float32)
    result += jnp.dot(place[1], y, preferred_element_type=jnp.float32)
    result += jnp.dot(place[2], y, preferred_element_type=jnp.float32)
    out_ref[...] = result.astype(out_ref.dtype)

    for k in range(CHUNKS):
        each(n_ep - 1, lambda j: send_tokens(k, j).wait_send())
    for c in sends:
        c.wait_send()
    each(n_ep - 1, lambda j: send_back(j).wait_send())


def local(tokens, chosen, chosen_weight, gate_weight, up_weight, down_weight):
    n_ep, n_tp = lax.axis_size("ep"), lax.axis_size("tp")
    tok_count, width = tokens.shape
    blocks, experts, picks = chosen.shape
    hid = gate_weight.shape[2]
    rows = blocks * picks
    cw, sw = width // CHUNKS, width // n_tp
    bf, f32 = jnp.bfloat16, jnp.float32
    dma = pltpu.SemaphoreType.DMA
    hbm = pl.BlockSpec(memory_space=pl.ANY)
    return pl.pallas_call(
        functools.partial(kernel, n_ep, n_tp),
        out_shape=jax.ShapeDtypeStruct((tok_count, sw), bf),
        in_specs=[hbm] * 6,
        out_specs=pl.BlockSpec(memory_space=pltpu.VMEM),
        scratch_shapes=[
            pltpu.VMEM((tok_count, width), bf),
            pltpu.VMEM((experts, picks), jnp.int32),
            pltpu.VMEM((experts, picks), f32),
            pltpu.VMEM((width, hid), bf),
            pltpu.VMEM((width, hid), bf),
            pltpu.VMEM((n_tp, hid, sw), bf),
            pltpu.VMEM((CHUNKS, experts, picks, cw), bf),
            pltpu.VMEM((CHUNKS, blocks, picks, cw), bf),
            pltpu.VMEM((rows, hid), f32),
            pltpu.VMEM((rows, hid), f32),
            pltpu.VMEM((3, tok_count, experts * picks), bf),
            pltpu.VMEM((n_tp, rows, sw), bf),
            pltpu.VMEM((n_tp - 1, rows, sw), bf),
            pltpu.VMEM((blocks, picks, sw), bf),
            pltpu.VMEM((experts, picks, sw), bf),
            dma((3,)),
            dma((2, CHUNKS)),
            dma((n_tp,)),
            dma((CHUNKS, n_ep)),
            dma((CHUNKS, n_ep)),
            dma((n_tp,)),
            dma((n_tp,)),
            dma((n_ep,)),
            dma((n_ep,)),
        ],
        compiler_params=pltpu.CompilerParams(
            collective_id=0, has_side_effects=True, vmem_limit_bytes=60 * 1024 * 1024
        ),
    )(tokens, chosen, chosen_weight, gate_weight, up_weight, down_weight)


def solution(mesh):
    return jax.shard_map(
        local,
        mesh=mesh,
        in_specs=(
            P("ep", None),
            P(),
            P("ep", None, None),
            P("ep", None, "tp"),
            P("ep", None, "tp"),
            P("ep", "tp", None),
        ),
        out_specs=P("ep", "tp"),
        check_vma=False,
    )
```

time: 85.3 us -> 27.2 us (0.32)
  waiting for transfers between devices: 30.7 us -> 0 us
  Pallas kernels: 0 us -> 25.4 us
  between operations: 13.4 us -> 0.01 us
  starting transfers between devices: 11 us -> 0 us
  matrix products: 10.3 us -> 0 us
  blocking collectives: 8.98 us -> 0 us
  local copies, waits for them, and re-layouts: 8.96 us -> 1.57 us
  other arithmetic: 1.48 us -> 0 us
    pallas_call x0 -> x1, Pallas kernels: none -> 25.4 us  [local(): pl.pallas_call(functools.partial(kernel, n_ep, n_tp), out_shape=jax.Shape...]
    unnamed x2 -> x0, waiting for transfers between devices: 25 us -> none
    all_to_all x2 -> x0, starting transfers between devices: 11 us -> none  [the longest x1 6.35 us: local(): lax.all_to_all(leaving, 'ep', split_axis=0, concat_axis=0, tiled=True)]
    dot_general x3 -> x0, matrix products: 10.3 us -> none  [the longest x1 6.33 us: local(): jnp.einsum('rf,fcd->crd', hidden, down_local, preferred_element_type=jnp....]
    all_gather x1 -> x0, blocking collectives: 8.98 us -> none  [local(): portion = lax.all_gather(arrived, 'tp', axis=1, tiled=True)]
    another operation x1 -> x0, local copies, waits for them, and re-layouts: 7.8 us -> none  [local(): down_weight[0].reshape(down_weight.shape[1], tp_count, slice_width)]
    all_to_all x2 -> x0, waiting for transfers between devices: 5.76 us -> none  [the longest x1 5.76 us: local(): lax.all_to_all(expert_out, 'ep', split_axis=0, concat_axis=0, tiled=True)]
    unnamed x4 -> x1, local copies, waits for them, and re-layouts: 0.22 us -> 1.57 us
  transfers between devices with their start and end apart: 3 -> 0, of which waited for: 2 -> 0; matrix products, arithmetic and copies ran while one was open for 9% -> 0% of each run, Pallas kernels for 0% -> 0%
where the time goes in v1:
time: 27.2 us; the launch traced here: 27 us
  Pallas kernels  25.4 us (93%)
  local copies, waits for them, and re-layouts  1.57 us (6%)
    pallas_call x1, Pallas kernels, local(): pl.pallas_call(functools.partial(kernel, n_ep, n_tp), out_shape=jax.Shape...  25.4 us
    unnamed x1, local copies, waits for them, and re-layouts  1.57 us

profile of v1, /device:TPU:0, one launch (start us, length us, event | category | flops | bytes accessed | tf_op | source)
XLA Modules:
  0.0 27.0 jit_solution(12622882173610851357)
XLA Ops:
  0.0 25.4 %shard_map.64 = bf16[128,512]{1,0:T(8,128)(2,1)} custom-call(bf16[128,2048]{1,0:T(8,128)(2,1)} %tok_hbm.1, s32[8,8,8]{2,1,0:T(8,128)} %cho_hbm.1, f32[1,8,8]{2,1,0:T(8,128)} %wt_hbm.1, bf16[1,2048,1024]{2,1,0:T(8,128)(2,1)} %gate_hbm.1, bf16[1,2048,1024]{2,1,0:T(8,128)(2,1)} %up_hbm.1, bf16[1,1024,2048]{2,1,0:T(8,128)(2,1)} %down_hbm.1), custom_call_target="tpu_custom_call" | custom-call | tf_op jit(solution)/shard_map/pallas_call | solution.py:226
  25.4 1.6 %copy.8 = bf16[128,512]{1,0:T(8,128)(2,1)} copy(bf16[128,512]{1,0:T(8,128)(2,1)} %shard_map.64) | data formatting | bytes 262144

commit v2 on v1

--- a/solution.py
+++ b/solution.py
@@ -78,8 +78,6 @@
         piece = pl.ds(k * cw, cw)
         a = pltpu.make_async_copy(gate_hbm.at[0, piece, :], gate.at[piece, :], w_sem.at[0, k])
         b = pltpu.make_async_copy(up_hbm.at[0, piece, :], up.at[piece, :], w_sem.at[1, k])
-        a.start()
-        b.start()
         wloads.append((a, b))
     order = [*range(n_tp - 1, 0, -1), 0]
     dloads = {}
@@ -88,7 +86,6 @@
         dloads[j] = pltpu.make_async_copy(
             down_hbm.at[0, :, pl.ds(col, sw)], down.at[j], d_sem.at[j]
         )
-        dloads[j].start()
 
     for c in loads:
         c.wait()
@@ -127,6 +124,11 @@
 
     for k in range(CHUNKS):
         each(n_ep - 1, lambda j: send_tokens(k, j).start())
+    for a, b in wloads:
+        a.start()
+        b.start()
+    for j in order:
+        dloads[j].start()
 
     weighted = jnp.concatenate(parts, axis=0)
     hi = weighted.astype(jnp.bfloat16).astype(jnp.float32)
@@ -222,7 +224,7 @@
     cw, sw = width // CHUNKS, width // n_tp
     bf, f32 = jnp.bfloat16, jnp.float32
     dma = pltpu.SemaphoreType.DMA
-    hbm = pl.BlockSpec(memory_space=pl.ANY)
+    hbm = pl.BlockSpec(memory_space=pltpu.HBM)
     return pl.pallas_call(
         functools.partial(kernel, n_ep, n_tp),
         out_shape=jax.ShapeDtypeStruct((tok_count, sw), bf),
@@ -255,9 +257,12 @@
             dma((n_ep,)),
         ],
         compiler_params=pltpu.CompilerParams(
-            collective_id=0, has_side_effects=True, vmem_limit_bytes=60 * 1024 * 1024
+            collective_id=0, has_side_effects=True, vmem_limit_bytes=32 * 1024 * 1024
         ),
-    )(tokens, chosen, chosen_weight, gate_weight, up_weight, down_weight)
+    )(*(
+        pltpu.with_memory_space_constraint(a, pltpu.HBM)
+        for a in (tokens, chosen, chosen_weight, gate_weight, up_weight, down_weight)
+    ))
 
 
 def solution(mesh):

time: 27.2 us -> 24.2 us (0.89)
  Pallas kernels: 25.4 us -> 23.4 us
  local copies, waits for them, and re-layouts: 1.57 us -> 0.66 us
    pallas_call x1, Pallas kernels: 25.4 us -> 23.4 us  [local(): pl.pallas_call(functools.partial(kernel, n_ep, n_tp), out_shape=jax.Shape...]
    unnamed x1, local copies, waits for them, and re-layouts: 1.57 us -> 0.66 us
where the time goes in v2:
time: 24.2 us; the launch traced here: 24.1 us
  Pallas kernels  23.4 us (97%)
  local copies, waits for them, and re-layouts  0.66 us (3%)
    pallas_call x1, Pallas kernels, local(): pl.pallas_call(functools.partial(kernel, n_ep, n_tp), out_shape=jax.Shape...  23.4 us
    unnamed x1, local copies, waits for them, and re-layouts  0.66 us

profile of v2, /device:TPU:0, one launch (start us, length us, event | category | flops | bytes accessed | tf_op | source)
XLA Modules:
  0.0 24.1 jit_solution(9368036636885530469)
XLA Ops:
  0.0 23.4 %shard_map.64 = bf16[128,512]{1,0:T(8,128)(2,1)S(1)} custom-call(bf16[128,2048]{1,0:T(8,128)(2,1)} %tok_hbm.1, s32[8,8,8]{2,1,0:T(8,128)} %cho_hbm.1, f32[1,8,8]{2,1,0:T(8,128)} %wt_hbm.1, bf16[1,2048,1024]{2,1,0:T(8,128)(2,1)} %gate_hbm.1, bf16[1,2048,1024]{2,1,0:T(8,128)(2,1)} %up_hbm.1, bf16[1,1024,2048]{2,1,0:T(8,128)(2,1)} %down_hbm.1), custom_call_target="tpu_custom_call" | custom-call | tf_op jit(solution)/shard_map/pallas_call | solution.py:228
  23.4 0.7 %copy.8 = bf16[128,512]{1,0:T(8,128)(2,1)} copy(bf16[128,512]{1,0:T(8,128)(2,1)S(1)} %shard_map.64) | data formatting | bytes 262144

commit v3 on v2

--- a/solution.py
+++ b/solution.py
@@ -8,7 +8,7 @@
 from jax.sharding import PartitionSpec as P
 
 MESH = pl.DeviceIdType.MESH
-CHUNKS = 4
+CHUNKS = 2
 
 
 def each(count, body):
@@ -47,13 +47,14 @@
     rows = experts * picks
     cw = width // CHUNKS
     sw = width // n_tp
-    hid = gate.shape[1]
+    half = n_ep // 2
+    far = jnp.where(e < half, 1, 0)
 
     def ep_peer(j):
         low = n_ep - 1 - j
         low = jnp.where(low > e, low, low - 1)
         high = jnp.where(j < e, j, j + 1)
-        return jnp.where(e < n_ep // 2, low, high)
+        return jnp.where(e < half, low, high)
 
     barrier = pltpu.get_barrier_semaphore()
 
@@ -164,29 +165,16 @@
     g = gate_acc[...]
     hidden = (g / (1.0 + jnp.exp(-g)) * up_acc[...]).astype(jnp.bfloat16)
 
-    sends = []
-    for j in order:
-        dloads[j].wait()
-        part_out[j] = jnp.dot(hidden, down[j], preferred_element_type=jnp.float32).astype(
-            jnp.bfloat16
-        )
-        if j:
-            c = pltpu.make_async_remote_copy(
-                src_ref=part_out.at[j],
-                dst_ref=part_in.at[j - 1],
-                send_sem=s2_send.at[j - 1],
-                recv_sem=s2_recv.at[j - 1],
-                device_id={"tp": partner(t, j, n_tp)},
-                device_id_type=MESH,
-            )
-            c.start()
-            sends.append(c)
-    total = part_out[0].astype(jnp.float32)
-    for c in sends:
-        c.wait_recv()
-    for j in range(1, n_tp):
-        total += part_in[j - 1].astype(jnp.float32)
-    back_out[...] = total.reshape(n_ep, picks, sw).astype(jnp.bfloat16)
+    def send_part(h, j):
+        side = far if h == 0 else 1 - far
+        return pltpu.make_async_remote_copy(
+            src_ref=part_out.at[j, side],
+            dst_ref=part_in.at[j - 1, side],
+            send_sem=s2_send.at[h, j],
+            recv_sem=s2_recv.at[h, j],
+            device_id={"tp": partner(t, j, n_tp)},
+            device_id_type=MESH,
+        )
 
     def send_back(j):
         p = ep_peer(j)
@@ -199,7 +187,26 @@
             device_id_type=MESH,
         )
 
-    each(n_ep - 1, lambda j: send_back(j).start())
+    for j in order:
+        dloads[j].wait()
+        part = jnp.dot(hidden, down[j], preferred_element_type=jnp.float32)
+        part_out[j] = part.reshape(2, rows // 2, sw).astype(jnp.bfloat16)
+        if j:
+            send_part(0, j).start()
+        if j == 1:
+            for i in range(n_tp - 1, 0, -1):
+                send_part(1, i).start()
+    for h in range(2):
+        side = far if h == 0 else 1 - far
+        total = part_out[0, side].astype(jnp.float32)
+        for j in range(n_tp - 1, 0, -1):
+            send_part(h, j).wait_recv()
+            total += part_in[j - 1, side].astype(jnp.float32)
+        back_out[pl.ds(side * half, half)] = total.reshape(half, picks, sw).astype(jnp.bfloat16)
+        if h == 0:
+            each(half, lambda j: send_back(j).start())
+        else:
+            each(half - 1, lambda j: send_back(j + half).start())
     back_in[e] = back_out[e]
     each(n_ep - 1, lambda j: rows_in(back_in, None, s3_recv, ep_peer(j)))
     y = back_in[...].astype(jnp.float32).reshape(rows, sw).astype(jnp.bfloat16)
@@ -210,8 +217,9 @@
 
     for k in range(CHUNKS):
         each(n_ep - 1, lambda j: send_tokens(k, j).wait_send())
-    for c in sends:
-        c.wait_send()
+    for j in range(1, n_tp):
+        send_part(0, j).wait_send()
+        send_part(1, j).wait_send()
     each(n_ep - 1, lambda j: send_back(j).wait_send())
 
 
@@ -242,8 +250,8 @@
             pltpu.VMEM((rows, hid), f32),
             pltpu.VMEM((rows, hid), f32),
             pltpu.VMEM((3, tok_count, experts * picks), bf),
-            pltpu.VMEM((n_tp, rows, sw), bf),
-            pltpu.VMEM((n_tp - 1, rows, sw), bf),
+            pltpu.VMEM((n_tp, 2, rows // 2, sw), bf),
+            pltpu.VMEM((n_tp - 1, 2, rows // 2, sw), bf),
             pltpu.VMEM((blocks, picks, sw), bf),
             pltpu.VMEM((experts, picks, sw), bf),
             dma((3,)),
@@ -251,8 +259,8 @@
             dma((n_tp,)),
             dma((CHUNKS, n_ep)),
             dma((CHUNKS, n_ep)),
-            dma((n_tp,)),
-            dma((n_tp,)),
+            dma((2, n_tp)),
+            dma((2, n_tp)),
             dma((n_ep,)),
             dma((n_ep,)),
         ],

time: 24.2 us -> 23.5 us (0.971)
  Pallas kernels: 23.4 us -> 22.7 us
    pallas_call x1, Pallas kernels: 23.4 us -> 22.7 us  [local(): pl.pallas_call(functools.partial(kernel, n_ep, n_tp), out_shape=jax.Shape...]
where the time goes in v3:
time: 23.5 us; the launch traced here: 23.4 us
  Pallas kernels  22.7 us (97%)
  local copies, waits for them, and re-layouts  0.66 us (3%)
    pallas_call x1, Pallas kernels, local(): pl.pallas_call(functools.partial(kernel, n_ep, n_tp), out_shape=jax.Shape...  22.7 us
    unnamed x1, local copies, waits for them, and re-layouts  0.66 us

profile of v3, /device:TPU:0, one launch (start us, length us, event | category | flops | bytes accessed | tf_op | source)
XLA Modules:
  0.0 23.4 jit_solution(8032785235249993399)
XLA Ops:
  0.0 22.7 %shard_map.64 = bf16[128,512]{1,0:T(8,128)(2,1)S(1)} custom-call(bf16[128,2048]{1,0:T(8,128)(2,1)} %tok_hbm.1, s32[8,8,8]{2,1,0:T(8,128)} %cho_hbm.1, f32[1,8,8]{2,1,0:T(8,128)} %wt_hbm.1, bf16[1,2048,1024]{2,1,0:T(8,128)(2,1)} %gate_hbm.1, bf16[1,2048,1024]{2,1,0:T(8,128)(2,1)} %up_hbm.1, bf16[1,1024,2048]{2,1,0:T(8,128)(2,1)} %down_hbm.1), custom_call_target="tpu_custom_call" | custom-call | tf_op jit(solution)/shard_map/pallas_call | solution.py:236
  22.7 0.7 %copy.8 = bf16[128,512]{1,0:T(8,128)(2,1)} copy(bf16[128,512]{1,0:T(8,128)(2,1)S(1)} %shard_map.64) | data formatting | bytes 262144

commit v4 on v3

--- a/solution.py
+++ b/solution.py
@@ -193,9 +193,7 @@
         part_out[j] = part.reshape(2, rows // 2, sw).astype(jnp.bfloat16)
         if j:
             send_part(0, j).start()
-        if j == 1:
-            for i in range(n_tp - 1, 0, -1):
-                send_part(1, i).start()
+            send_part(1, j).start()
     for h in range(2):
         side = far if h == 0 else 1 - far
         total = part_out[0, side].astype(jnp.float32)
@@ -210,9 +208,9 @@
     back_in[e] = back_out[e]
     each(n_ep - 1, lambda j: rows_in(back_in, None, s3_recv, ep_peer(j)))
     y = back_in[...].astype(jnp.float32).reshape(rows, sw).astype(jnp.bfloat16)
-    result = jnp.dot(place[0], y, preferred_element_type=jnp.float32)
-    result += jnp.dot(place[1], y, preferred_element_type=jnp.float32)
-    result += jnp.dot(place[2], y, preferred_element_type=jnp.float32)
+    terms = jnp.concatenate([place[0], place[1], place[2]], axis=0)
+    terms = jnp.dot(terms, y, preferred_element_type=jnp.float32)
+    result = terms[:tok_count] + terms[tok_count : 2 * tok_count] + terms[2 * tok_count :]
     out_ref[...] = result.astype(out_ref.dtype)
 
     for k in range(CHUNKS):

time: 23.5 us -> 23.5 us (level)
  no operation moved by 1% of the time
where the time goes in v4:
time: 23.5 us; the launch traced here: 23.3 us
  Pallas kernels  22.7 us (97%)
  local copies, waits for them, and re-layouts  0.66 us (3%)
    pallas_call x1, Pallas kernels, local(): pl.pallas_call(functools.partial(kernel, n_ep, n_tp), out_shape=jax.Shape...  22.7 us
    unnamed x1, local copies, waits for them, and re-layouts  0.66 us

profile of v4, /device:TPU:0, one launch (start us, length us, event | category | flops | bytes accessed | tf_op | source)
XLA Modules:
  0.0 23.3 jit_solution(13675108544541042495)
XLA Ops:
  0.0 22.7 %shard_map.64 = bf16[128,512]{1,0:T(8,128)(2,1)S(1)} custom-call(bf16[128,2048]{1,0:T(8,128)(2,1)} %tok_hbm.1, s32[8,8,8]{2,1,0:T(8,128)} %cho_hbm.1, f32[1,8,8]{2,1,0:T(8,128)} %wt_hbm.1, bf16[1,2048,1024]{2,1,0:T(8,128)(2,1)} %gate_hbm.1, bf16[1,2048,1024]{2,1,0:T(8,128)(2,1)} %up_hbm.1, bf16[1,1024,2048]{2,1,0:T(8,128)(2,1)} %down_hbm.1), custom_call_target="tpu_custom_call" | custom-call | tf_op jit(solution)/shard_map/pallas_call | solution.py:234
  22.7 0.7 %copy.8 = bf16[128,512]{1,0:T(8,128)(2,1)} copy(bf16[128,512]{1,0:T(8,128)(2,1)S(1)} %shard_map.64) | data formatting | bytes 262144
